TPU v7x, 32 devices: a whole 2x2x4 slice. The times are simulated.
32 devices in a mesh: dp: 2 (over x), kv: 8 (over z, y), tp: 2 (over core).
Axes of the slice: x: 2, y: 2, z: 4, core: 2. Of those that a mesh axis runs over, the one named last changes fastest.
Arguments:
- tokens: bfloat16 [2, 1536, 2048], P('dp', 'kv'), may hold values from -60 to 60
- doc_lengths: int32 [2, 8], P('dp'), may hold values from 1 to 768, as said below
- picked: int32 [2, 48, 32], P('dp', 'kv'), may hold values from -1 to 47, as said below
- w_query: bfloat16 [2048, 1024], P(None, 'tp'), may hold values from -0.125 to 0.125
- w_key: bfloat16 [2048, 128], replicated, may hold values from -0.125 to 0.125
- w_value: bfloat16 [2048, 128], replicated, may hold values from -0.125 to 0.125
- w_out: bfloat16 [1024, 2048], replicated, may hold values from -0.1875 to 0.1875
Outputs:
- mixed: bfloat16 [2, 1536, 2048], P('dp', 'kv')
Inputs may be any that keep to these rules, and one draw needn't show every extreme that they name: `doc_lengths`: each row sums to 1536; its largest document has exactly 768 positions. `picked`: slot 0 of query block b is b itself; the other slots hold distinct blocks before b, or -1 when fewer such blocks are named. Of the 6 blocks that one device of kv holds, at most 2 are named by query blocks held by other devices of kv, and in every row some device reaches 2.
All inputs are finite; a program needn't handle non-finite values.
Results may differ from a plain program's by a relative error of at most 0.011.
Values may be sent and summed in bfloat16 or wider, within the bound.
A program may use at most 64 MiB of HBM per device.

v0:
```python
import jax
import jax.numpy as jnp
from jax import lax
from jax.sharding import PartitionSpec as P

KV_HEADS = 2
HEAD_DIM = 64
BLOCK = 32
PICKS = 32


def rotate(values_in, positions):
    half = values_in.shape[-1] // 2
    inverse = 10000.0 ** (-jnp.arange(half, dtype=jnp.float32) / half)
    angles = positions.astype(jnp.float32)[:, None] * inverse[None, :]
    cosine = jnp.cos(angles)[:, None, :]
    sine = jnp.sin(angles)[:, None, :]
    first = values_in[..., :half]
    second = values_in[..., half:]
    return jnp.concatenate(
        [first * cosine - second * sine, second * cosine + first * sine], axis=-1
    )


def doc_of(positions, ends):
    return jnp.sum((positions[..., None] >= ends).astype(jnp.int32), axis=-1)


def shards(tokens, doc_lengths, picked, w_query, w_key, w_value, w_out):
    local = tokens[0]
    rows = local.shape[0]
    kv_index = lax.axis_index("kv")
    tp_index = lax.axis_index("tp")
    positions = kv_index * rows + jnp.arange(rows, dtype=jnp.int32)
    heads_dev = w_query.shape[1] // HEAD_DIM
    kv_dev = KV_HEADS // lax.axis_size("tp")
    group = heads_dev // kv_dev
    width = kv_dev * HEAD_DIM
    queries = rotate(
        jnp.dot(local, w_query, preferred_element_type=jnp.float32).reshape(
            rows, heads_dev, HEAD_DIM
        ),
        positions,
    ).astype(jnp.bfloat16)
    key_cols = lax.dynamic_slice_in_dim(w_key, tp_index * width, width, 1)
    value_cols = lax.dynamic_slice_in_dim(w_value, tp_index * width, width, 1)
    keys = rotate(
        jnp.dot(local, key_cols, preferred_element_type=jnp.float32).reshape(
            rows, kv_dev, HEAD_DIM
        ),
        positions,
    ).astype(jnp.bfloat16)
    values = jnp.dot(local, value_cols, preferred_element_type=jnp.float32).astype(jnp.bfloat16)
    packed = jnp.concatenate([keys.reshape(rows, width), values], axis=1)
    ends = jnp.cumsum(doc_lengths[0])
    blocks_dev = rows // BLOCK
    slots = picked[0]
    offsets = jnp.arange(BLOCK, dtype=jnp.int32)
    chosen = jnp.maximum(slots, 0)
    key_pos = (chosen[:, :, None] * BLOCK + offsets[None, None, :]).reshape(
        blocks_dev, PICKS * BLOCK
    )
    every = lax.all_gather(packed, "kv", axis=0, tiled=True)
    selected = every[key_pos]
    block_keys = selected[..., :width].reshape(blocks_dev, PICKS * BLOCK, kv_dev, HEAD_DIM)
    block_values = selected[..., width:].reshape(blocks_dev, PICKS * BLOCK, kv_dev, HEAD_DIM)
    query_pos = positions.reshape(blocks_dev, BLOCK)
    filled = jnp.repeat(slots >= 0, BLOCK, axis=1)
    live = (
        filled[:, None, :]
        & (key_pos[:, None, :] <= query_pos[:, :, None])
        & (doc_of(key_pos, ends)[:, None, :] == doc_of(query_pos, ends)[:, :, None])
    )
    grouped = queries.reshape(blocks_dev, BLOCK, kv_dev, group, HEAD_DIM)
    scores = jnp.einsum(
        "bqngd,bknd->bngqk", grouped, block_keys, preferred_element_type=jnp.float32
    ) * HEAD_DIM ** (-0.5)
    scores = jnp.where(live[:, None, None], scores, -jnp.inf)
    highest = jnp.max(scores, axis=-1, keepdims=True)
    weights = jnp.exp(scores - highest)
    total = jnp.sum(weights, axis=-1)
    summed = jnp.einsum(
        "bngqk,bknd->bqngd",
        weights.astype(jnp.bfloat16),
        block_values,
        preferred_element_type=jnp.float32,
    )
    result = summed / jnp.transpose(total, (0, 3, 1, 2))[..., None]
    attended = result.astype(jnp.bfloat16).reshape(rows, heads_dev * HEAD_DIM)
    whole = lax.all_gather(attended, "tp", axis=1, tiled=True)
    mixed = jnp.dot(whole, w_out, preferred_element_type=jnp.float32).astype(jnp.bfloat16)
    return mixed[None]


def solution(mesh):
    placed = (P("dp", "kv", None), P("dp", None), P("dp", "kv", None), P(None, "tp"), P(), P(), P())
    return jax.shard_map(
        shards, mesh=mesh, in_specs=placed, out_specs=P("dp", "kv", None), check_vma=False
    )
```

profile of v0, /device:TPU:0, one launch (start us, length us, event | category | flops | bytes accessed | tf_op | source)
XLA Modules:
  0.0 83.3 jit_solution(2517462831864149929)
XLA Ops:
  0.0 0.9 %reduce-window.8 = s32[8,1]{0,1:T(1,128)S(1)} reduce-window(s32[8,1]{0,1:T(1,128)} %bitcast.114, s32[]{:T(128)} %constant.13.clone.1), window={size=8x1 pad=7_0x0_0}, to_apply=%region_0.0 | reduce-window | flops 56 | bytes 68 | tf_op jit(solution)/shard_map/reduce-window.3
  0.9 0.7 broadcast_compare_fusion
  1.6 0.7 maximum_multiply_fusion
  2.7 1.7 %fusion.15 = bf16[192,64]{0,1:T(8,128)(2,1)S(1)} fusion(bf16[1,192,2048]{2,1,0:T(8,128)(2,1)S(1)} %copy-done, bf16[2048,128]{1,0:T(8,128)(2,1)} %param.12, s32[]{:T(128)S(6)} %select_n.18), kind=kOutput, calls=%fused_computation.20 | convolution fusion | flops 50343936 | bytes 1335300 | tf_op jit(solution)/shard_map/dot_general | solution.py:53
  4.4 1.6 %convolution_bitcast_fusion = f32[192,1,64]{0,2,1:T(8,128)S(1)} fusion(bf16[1,192,2048]{2,1,0:T(8,128)(2,1)S(1)} %copy-done, bf16[2048,128]{1,0:T(8,128)(2,1)} %param.11, s32[]{:T(128)S(6)} %select_n.18), kind=kOutput, calls=%fused_computation.18 | convolution fusion | flops 50331648 | bytes 1359876 | tf_op jit(solution)/shard_map/dot_general | solution.py:48
  6.1 0.2 fusion.40
  6.4 0.8 multiply_cosine_fusion
  7.6 0.1 convert_reduce_fusion
  7.7 0.4 compare_and_fusion
  8.1 32.8 %all_gather.6 = bf16[1536,128]{1,0:T(8,128)(2,1)S(1)} all-gather(bf16[192,128]{1,0:T(8,128)(2,1)S(1)} %copy.26), channel_id=1, replica_groups=mesh['dp'=2,'kv'=8,'tp'=2] {'kv'}, dimensions={0}, use_global_device_ids=true | all-gather | bytes 442368 | tf_op jit(solution)/shard_map/all_gather | solution.py:63
  40.9 22.0 %gather_fusion = bf16[6144,128]{1,0:T(8,128)(2,1)} fusion(bf16[1536,128]{1,0:T(8,128)(2,1)S(1)} %all_gather.6, s32[6144]{0:T(1024)S(1)} %broadcast_clamp_fusion), kind=kCustom, calls=%fused_computation | custom fusion | bytes 3170304 | tf_op jit(solution)/shard_map/gather | solution.py:64
  62.9 2.5 %copy.29 = bf16[2048,512]{0,1:T(8,128)(2,1)} copy(bf16[2048,512]{1,0:T(8,128)(2,1)S(1)} %copy-done.1) | data formatting | bytes 4194304 | tf_op args[3]
  65.4 2.4 %fusion.22 = f32[192,8,64]{0,2,1:T(8,128)S(1)} fusion(bf16[8,64,2048]{2,1,0:T(8,128)(2,1)} %bitcast.106, bf16[1,192,2048]{2,1,0:T(8,128)(2,1)S(1)} %copy-done), kind=kOutput, calls=%fused_computation.23 | convolution fusion | flops 402653184 | bytes 3276800 | tf_op jit(solution)/shard_map/dot_general | solution.py:40
  67.9 0.3 concatenate.26
  68.2 1.1 %copy.30 = bf16[6,32,8,32]{3,1,2,0:T(8,128)(2,1)} copy(bf16[6,32,8,32]{1,0,3,2:T(8,128)(2,1)S(1)} %concatenate.26) | data formatting | bytes 196608 | tf_op jit(solution)/shard_map/concatenate | solution.py:20
  69.3 0.3 concatenate.27
  69.5 1.1 %copy.31 = bf16[6,32,8,32]{3,1,2,0:T(8,128)(2,1)} copy(bf16[6,32,8,32]{1,0,3,2:T(8,128)(2,1)S(1)} %concatenate.27) | data formatting | bytes 196608 | tf_op jit(solution)/shard_map/concatenate | solution.py:20
  70.6 2.3 %fusion.2 = (f32[6,8,32]{2,1,0:T(8,128)S(1)}, f32[6,1024,32,8]{1,2,3,0:T(8,128)S(1)}) fusion(pred[6,32,1024]{2,1,0:T(8,128)(4,1)S(1)} %compare_and_fusion, bf16[6,32,8,32]{3,1,2,0:T(8,128)(2,1)} %copy.31, bf16[6,32,8,32]{3,1,2,0:T(8,128)(2,1)} %copy.30, bf16[6,1024,128]{2,1,0:T(8,128)(2,1)S(1)} %bitcast.107), kind=kOutput, calls=%fused_computation.5 | convolution fusion | flops 206436864 | bytes 8263680 | tf_op jit(solution)/shard_map/bqngd,bknd->bngqk/dot_general | solution.py:75
  72.9 1.6 %fusion = f32[6,8,32]{2,1,0:T(8,128)S(1)} fusion(f32[6,1024,32,8]{1,2,3,0:T(8,128)S(1)} %get-tuple-element.12, f32[6,8,32]{2,1,0:T(8,128)S(1)} %get-tuple-element.11, pred[6,32,1024]{2,1,0:T(8,128)(4,1)S(1)} %compare_and_fusion), kind=kLoop, calls=%fused_computation.3 | loop fusion | flops 6289920 | bytes 6500352 | tf_op jit(solution)/shard_map/reduce_sum | solution.py:81
  74.6 2.1 %fusion.19 = bf16[6,32,1,8,64]{4,1,3,0,2:T(8,128)(2,1)S(1)} fusion(f32[6,1024,32,8]{1,2,3,0:T(8,128)S(1)} %get-tuple-element.12, f32[6,8,32]{2,1,0:T(8,128)S(1)} %get-tuple-element.11, pred[6,32,1024]{2,1,0:T(8,128)(4,1)S(1)} %compare_and_fusion, bf16[6,1024,128]{2,1,0:T(8,128)(2,1)S(1)} %bitcast.108, f32[6,32,8]{1,2,0:T(8,128)S(1)} %bitcast.109), kind=kOutput, calls=%fused_computation.22 | convolution fusion | flops 207814656 | bytes 8269824 | tf_op jit(solution)/shard_map/bngqk,bknd->bqngd/dot_general | solution.py:82
  76.7 0.2 copy.32
  76.9 0.3 reshape.293
  77.1 2.1 %all_gather.7 = bf16[192,1024]{1,0:T(8,128)(2,1)S(1)} all-gather(bf16[192,512]{1,0:T(8,128)(2,1)S(1)} %reshape.293), channel_id=1, replica_groups=mesh['dp'=2,'kv'=8,'tp'=2] {'tp'}, dimensions={1}, use_global_device_ids=true | all-gather | bytes 589824 | tf_op jit(solution)/shard_map/all_gather | solution.py:90
  79.2 4.1 %fusion.10 = bf16[1,192,2048]{2,1,0:T(8,128)(2,1)} fusion(bf16[192,1024]{1,0:T(8,128)(2,1)S(1)} %all_gather.7, bf16[1024,2048]{1,0:T(8,128)(2,1)} %param.13), kind=kOutput, calls=%fused_computation.13 | convolution fusion | flops 805699584 | bytes 5373952 | tf_op jit(solution)/shard_map/dot_general | solution.py:91
  (28 shorter events, 0.9 us)
Async XLA Ops:
  0.0 2.7 %copy-start = (bf16[1,192,2048]{2,1,0:T(8,128)(2,1)S(1)}, bf16[1,192,2048]{2,1,0:T(8,128)(2,1)}, u32[]{:S(2)}) copy-start(bf16[1,192,2048]{2,1,0:T(8,128)(2,1)} %param.7) | copy-start | bytes 2359300
  40.9 22.0 %copy-start.1 = (bf16[2048,512]{1,0:T(8,128)(2,1)S(1)}, bf16[2048,512]{1,0:T(8,128)(2,1)}, u32[]{:S(2)}) copy-start(bf16[2048,512]{1,0:T(8,128)(2,1)} %param.10) | copy-start | bytes 6291460
  62.9 4.9 %copy-start.3 = (f32[192,32]{0,1:T(8,128)S(1)}, f32[192,32]{0,1:T(8,128)}, u32[]{:S(2)}) copy-start(f32[192,32]{0,1:T(8,128)} %get-tuple-element.10) | copy-start | bytes 73732
  65.4 5.2 %copy-start.2 = (bf16[6144,128]{1,0:T(8,128)(2,1)S(1)}, bf16[6144,128]{1,0:T(8,128)(2,1)}, u32[]{:S(2)}) copy-start(bf16[6144,128]{1,0:T(8,128)(2,1)} %gather_fusion) | copy-start | bytes 4718596
where the time goes:
time: 83.7 us; the launch traced here: 83.3 us
  blocking collectives  34.9 us (42%)
  local copies, waits for them, and re-layouts  28.3 us (34%)
  matrix products  14.3 us (17%)
  other arithmetic  5.67 us (7%)
    all_gather x1, blocking collectives, shards(): every = lax.all_gather(packed, 'kv', axis=0, tiled=True)  32.8 us
    gather x1, local copies, waits for them, and re-layouts, shards(): selected = every[key_pos]  22 us
    dot_general x1, matrix products, shards(): jnp.dot(whole, w_out, preferred_element_type=jnp.float32)  4.07 us
    concatenate x4, local copies, waits for them, and re-layouts, rotate(): jnp.concatenate([first * cosine - second * sine, second * cosine + first...  2.67 us
    unnamed x11, local copies, waits for them, and re-layouts  2.5 us
    dot_general x1, matrix products, shards(): jnp.dot(local, w_query, preferred_element_type=jnp.float32)  2.44 us
    dot_general x1, matrix products, shards(): jnp.einsum('bqngd,bknd->bngqk', grouped, block_keys, preferred_element_ty...  2.3 us
    dot_general x1, matrix products, shards(): jnp.einsum('bngqk,bknd->bqngd', weights.astype(jnp.bfloat16), block_value...  2.13 us

commit v1 on v0

--- a/solution.py
+++ b/solution.py
@@ -60,7 +60,12 @@
     key_pos = (chosen[:, :, None] * BLOCK + offsets[None, None, :]).reshape(
         blocks_dev, PICKS * BLOCK
     )
-    every = lax.all_gather(packed, "kv", axis=0, tiled=True)
+    ring = [packed]
+    for hop in range(7):
+        ring.append(lax.ppermute(ring[-1], "kv", [(dev, (dev + 1) % 8) for dev in range(8)]))
+    every = jnp.roll(
+        jnp.concatenate(ring[::-1], axis=0), (lax.axis_index("kv") + 1) * ring[0].shape[0], axis=0
+    )
     selected = every[key_pos]
     block_keys = selected[..., :width].reshape(blocks_dev, PICKS * BLOCK, kv_dev, HEAD_DIM)
     block_values = selected[..., width:].reshape(blocks_dev, PICKS * BLOCK, kv_dev, HEAD_DIM)

time: 83.7 us -> 88.4 us (1.056)
  waiting for transfers between devices: 0 us -> 37.1 us
  blocking collectives: 34.9 us -> 2.09 us
  starting transfers between devices: 0 us -> 4.58 us
  local copies, waits for them, and re-layouts: 28.3 us -> 26.2 us
  other arithmetic: 5.67 us -> 3.63 us
    ppermute x0 -> x7, waiting for transfers between devices: none -> 37.1 us  [shards(): lax.ppermute(ring[-1], 'kv', [(dev, (dev + 1) % 8) for dev in range(8)])]
    all_gather x1 -> x0, blocking collectives: 32.8 us -> none  [shards(): every = lax.all_gather(packed, 'kv', axis=0, tiled=True)]
    ppermute x0 -> x7, starting transfers between devices: none -> 4.58 us  [shards(): lax.ppermute(ring[-1], 'kv', [(dev, (dev + 1) % 8) for dev in range(8)])]
    gather x1, local copies, waits for them, and re-layouts: 22 us -> 18.1 us  [shards(): selected = every[key_pos]]
    unnamed x11, local copies, waits for them, and re-layouts: 2.5 us -> 3.59 us
  transfers between devices with their start and end apart: 0 -> 7, of which waited for: 0 -> 6; matrix products, arithmetic and copies ran while one was open for 0% -> 11% of each run, Pallas kernels for 0% -> 0%
where the time goes in v1:
time: 88.4 us; the launch traced here: 88.1 us
  waiting for transfers between devices  37.1 us (42%)
  local copies, waits for them, and re-layouts  26.2 us (30%)
  matrix products  14.2 us (16%)
  starting transfers between devices  4.58 us (5%)
  other arithmetic  3.63 us (4%)
  blocking collectives  2.09 us (2%)
    ppermute x7, waiting for transfers between devices, shards(): lax.ppermute(ring[-1], 'kv', [(dev, (dev + 1) % 8) for dev in range(8)])  37.1 us
    gather x1, local copies, waits for them, and re-layouts, shards(): selected = every[key_pos]  18.1 us
    ppermute x7, starting transfers between devices, shards(): lax.ppermute(ring[-1], 'kv', [(dev, (dev + 1) % 8) for dev in range(8)])  4.58 us
    dot_general x1, matrix products, shards(): jnp.dot(whole, w_out, preferred_element_type=jnp.float32)  4.08 us
    unnamed x11, local copies, waits for them, and re-layouts  3.59 us
    concatenate x4, local copies, waits for them, and re-layouts, rotate(): jnp.concatenate([first * cosine - second * sine, second * cosine + first...  2.66 us
    dot_general x1, matrix products, shards(): jnp.dot(local, w_query, preferred_element_type=jnp.float32)  2.32 us
    dot_general x1, matrix products, shards(): jnp.einsum('bqngd,bknd->bngqk', grouped, block_keys, preferred_element_ty...  2.31 us
  transfers between devices with their start and end apart: 7, of which 6 were waited for; matrix products, arithmetic and copies ran while one was open for 11% of the time, Pallas kernels for 0%

profile of v1, /device:TPU:0, one launch (start us, length us, event | category | flops | bytes accessed | tf_op | source)
XLA Modules:
  0.0 88.1 jit_solution(7460922674338695233)
XLA Ops:
  0.0 1.1 %copy-done = bf16[1,192,2048]{2,1,0:T(8,128)(2,1)S(1)} copy-done((bf16[1,192,2048]{2,1,0:T(8,128)(2,1)S(1)}, bf16[1,192,2048]{2,1,0:T(8,128)(2,1)}, u32[]{:S(2)}) %copy-start) | copy-done | bytes 786456
  1.1 1.7 %fusion.15 = bf16[192,64]{0,1:T(8,128)(2,1)S(1)} fusion(bf16[1,192,2048]{2,1,0:T(8,128)(2,1)S(1)} %copy-done, bf16[2048,128]{1,0:T(8,128)(2,1)} %param.12, s32[]{:T(128)S(6)} %select_n.31), kind=kOutput, calls=%fused_computation.20 | convolution fusion | flops 50343936 | bytes 1335300 | tf_op jit(solution)/shard_map/dot_general | solution.py:53
  2.8 1.7 %convolution_bitcast_fusion = f32[192,1,64]{0,2,1:T(8,128)S(1)} fusion(bf16[1,192,2048]{2,1,0:T(8,128)(2,1)S(1)} %copy-done, bf16[2048,128]{1,0:T(8,128)(2,1)} %param.11, s32[]{:T(128)S(6)} %select_n.31), kind=kOutput, calls=%fused_computation.18 | convolution fusion | flops 50331648 | bytes 1359876 | tf_op jit(solution)/shard_map/dot_general | solution.py:48
  4.7 3.0 %collective-permute-start = (bf16[192,128]{0,1:T(8,128)(2,1)S(1)}, bf16[192,128]{0,1:T(8,128)(2,1)S(1)}, u32[]{:S(2)}, u32[]{:S(2)}) collective-permute-start(bf16[192,128]{0,1:T(8,128)(2,1)S(1)} %pad_maximum_fusion), channel_id=1, source_target_pairs={{0,2},{2,4},{4,6},{6,8},{8,10},{10,12},{12,14},{14,0},{1,3},{3,5},... | collective-permute-start | bytes 147464 | tf_op jit(solution)/shard_map/ppermute | solution.py:65
  8.0 0.7 maximum_multiply_fusion
  9.0 2.5 %copy.22 = bf16[2048,512]{0,1:T(8,128)(2,1)} copy(bf16[2048,512]{1,0:T(8,128)(2,1)S(1)} %copy-done.1) | data formatting | bytes 4194304 | tf_op args[3]
  11.4 2.3 %fusion.22 = f32[192,8,64]{0,2,1:T(8,128)S(1)} fusion(bf16[8,64,2048]{2,1,0:T(8,128)(2,1)} %bitcast.106, bf16[1,192,2048]{2,1,0:T(8,128)(2,1)S(1)} %copy-done), kind=kOutput, calls=%fused_computation.23 | convolution fusion | flops 402653184 | bytes 3276800 | tf_op jit(solution)/shard_map/dot_general | solution.py:40
  14.1 1.5 %collective-permute-start.1 = (bf16[192,128]{0,1:T(8,128)(2,1)S(1)}, bf16[192,128]{0,1:T(8,128)(2,1)S(1)}, u32[]{:S(2)}, u32[]{:S(2)}) collective-permute-start(bf16[192,128]{0,1:T(8,128)(2,1)S(1)} %collective-permute-done), channel_id=1, source_target_pairs={{0,2},{2,4},{4,6},{6,8},{8,10},{10,12},{12,14},{14,0},{1,3},{3,5},... | collective-permute-start | bytes 147464 | tf_op jit(solution)/shard_map/ppermute | solution.py:65
  15.7 5.3 %collective-permute-done.1 = bf16[192,128]{0,1:T(8,128)(2,1)S(1)} collective-permute-done((bf16[192,128]{0,1:T(8,128)(2,1)S(1)}, bf16[192,128]{0,1:T(8,128)(2,1)S(1)}, u32[]{:S(2)}, u32[]{:S(2)}) %collective-permute-start.1) | collective-permute-done | bytes 49184 | tf_op jit(solution)/shard_map/ppermute | solution.py:65
  21.0 7.0 %collective-permute-done.2 = bf16[192,128]{0,1:T(8,128)(2,1)S(1)} collective-permute-done((bf16[192,128]{0,1:T(8,128)(2,1)S(1)}, bf16[192,128]{0,1:T(8,128)(2,1)S(1)}, u32[]{:S(2)}, u32[]{:S(2)}) %collective-permute-start.2) | collective-permute-done | bytes 49184 | tf_op jit(solution)/shard_map/ppermute | solution.py:65
  28.3 6.6 %collective-permute-done.3 = bf16[192,128]{0,1:T(8,128)(2,1)S(1)} collective-permute-done((bf16[192,128]{0,1:T(8,128)(2,1)S(1)}, bf16[192,128]{0,1:T(8,128)(2,1)S(1)}, u32[]{:S(2)}, u32[]{:S(2)}) %collective-permute-start.3) | collective-permute-done | bytes 49184 | tf_op jit(solution)/shard_map/ppermute | solution.py:65
  35.0 0.4 compare_and_fusion
  35.4 6.5 %collective-permute-done.4 = bf16[192,128]{0,1:T(8,128)(2,1)S(1)} collective-permute-done((bf16[192,128]{0,1:T(8,128)(2,1)S(1)}, bf16[192,128]{0,1:T(8,128)(2,1)S(1)}, u32[]{:S(2)}, u32[]{:S(2)}) %collective-permute-start.4) | collective-permute-done | bytes 49184 | tf_op jit(solution)/shard_map/ppermute | solution.py:65
  42.0 7.4 %collective-permute-done.5 = bf16[192,128]{0,1:T(8,128)(2,1)S(1)} collective-permute-done((bf16[192,128]{0,1:T(8,128)(2,1)S(1)}, bf16[192,128]{0,1:T(8,128)(2,1)S(1)}, u32[]{:S(2)}, u32[]{:S(2)}) %collective-permute-start.5) | collective-permute-done | bytes 49184 | tf_op jit(solution)/shard_map/ppermute | solution.py:65
  49.7 1.1 %copy.23 = bf16[6,32,8,32]{3,1,2,0:T(8,128)(2,1)} copy(bf16[6,32,8,32]{1,0,3,2:T(8,128)(2,1)S(1)} %concatenate.33) | data formatting | bytes 196608 | tf_op jit(solution)/shard_map/concatenate | solution.py:20
  51.0 1.1 %copy.24 = bf16[6,32,8,32]{3,1,2,0:T(8,128)(2,1)} copy(bf16[6,32,8,32]{1,0,3,2:T(8,128)(2,1)S(1)} %concatenate.34) | data formatting | bytes 196608 | tf_op jit(solution)/shard_map/concatenate | solution.py:20
  52.1 4.2 %collective-permute-done.6 = bf16[192,128]{0,1:T(8,128)(2,1)S(1)} collective-permute-done((bf16[192,128]{0,1:T(8,128)(2,1)S(1)}, bf16[192,128]{0,1:T(8,128)(2,1)S(1)}, u32[]{:S(2)}, u32[]{:S(2)}) %collective-permute-start.6) | collective-permute-done | bytes 49184 | tf_op jit(solution)/shard_map/ppermute | solution.py:65
  56.4 0.5 concatenate.32
  57.3 18.1 %gather_fusion = bf16[6144,128]{1,0:T(8,128)(2,1)S(1)} fusion(bf16[1536,128]{1,0:T(8,128)(2,1)S(1)} %copy.19, s32[6144]{0:T(1024)S(1)} %broadcast_clamp_fusion), kind=kCustom, calls=%fused_computation | custom fusion | bytes 3170304 | tf_op jit(solution)/shard_map/gather | solution.py:69
  75.4 2.3 %fusion.2 = (f32[6,8,32]{2,1,0:T(8,128)S(1)}, f32[6,1024,32,8]{1,2,3,0:T(8,128)S(1)}) fusion(pred[6,32,1024]{2,1,0:T(8,128)(4,1)S(1)} %compare_and_fusion, bf16[6,32,8,32]{3,1,2,0:T(8,128)(2,1)} %copy.24, bf16[6,32,8,32]{3,1,2,0:T(8,128)(2,1)} %copy.23, bf16[6,1024,128]{2,1,0:T(8,128)(2,1)S(1)} %bitcast.107), kind=kOutput, calls=%fused_computation.5 | convolution fusion | flops 206436864 | bytes 8263680 | tf_op jit(solution)/shard_map/bqngd,bknd->bngqk/dot_general | solution.py:80
  77.7 1.6 %fusion = f32[6,8,32]{2,1,0:T(8,128)S(1)} fusion(f32[6,1024,32,8]{1,2,3,0:T(8,128)S(1)} %get-tuple-element.12, f32[6,8,32]{2,1,0:T(8,128)S(1)} %get-tuple-element.11, pred[6,32,1024]{2,1,0:T(8,128)(4,1)S(1)} %compare_and_fusion), kind=kLoop, calls=%fused_computation.3 | loop fusion | flops 6289920 | bytes 6500352 | tf_op jit(solution)/shard_map/reduce_sum | solution.py:86
  79.3 2.1 %fusion.19 = bf16[6,32,1,8,64]{4,1,3,0,2:T(8,128)(2,1)S(1)} fusion(f32[6,1024,32,8]{1,2,3,0:T(8,128)S(1)} %get-tuple-element.12, f32[6,8,32]{2,1,0:T(8,128)S(1)} %get-tuple-element.11, pred[6,32,1024]{2,1,0:T(8,128)(4,1)S(1)} %compare_and_fusion, bf16[6,1024,128]{2,1,0:T(8,128)(2,1)S(1)} %bitcast.108, f32[6,32,8]{1,2,0:T(8,128)S(1)} %bitcast.109), kind=kOutput, calls=%fused_computation.22 | convolution fusion | flops 207814656 | bytes 8269824 | tf_op jit(solution)/shard_map/bngqk,bknd->bqngd/dot_general | solution.py:87
  81.9 2.1 %all_gather.3 = bf16[192,1024]{1,0:T(8,128)(2,1)S(1)} all-gather(bf16[192,512]{1,0:T(8,128)(2,1)S(1)} %reshape.293), channel_id=1, replica_groups=mesh['dp'=2,'kv'=8,'tp'=2] {'tp'}, dimensions={1}, use_global_device_ids=true | all-gather | bytes 589824 | tf_op jit(solution)/shard_map/all_gather | solution.py:95
  84.0 4.1 %fusion.10 = bf16[1,192,2048]{2,1,0:T(8,128)(2,1)} fusion(bf16[192,1024]{1,0:T(8,128)(2,1)S(1)} %all_gather.3, bf16[1024,2048]{1,0:T(8,128)(2,1)} %param.13), kind=kOutput, calls=%fused_computation.13 | convolution fusion | flops 805699584 | bytes 5373952 | tf_op jit(solution)/shard_map/dot_general | solution.py:96
  (43 shorter events, 2.9 us)
Async XLA Ops:
  0.0 1.1 %copy-start = (bf16[1,192,2048]{2,1,0:T(8,128)(2,1)S(1)}, bf16[1,192,2048]{2,1,0:T(8,128)(2,1)}, u32[]{:S(2)}) copy-start(bf16[1,192,2048]{2,1,0:T(8,128)(2,1)} %param.7) | copy-start | bytes 2359300
  0.0 8.9 %copy-start.1 = (bf16[2048,512]{1,0:T(8,128)(2,1)S(1)}, bf16[2048,512]{1,0:T(8,128)(2,1)}, u32[]{:S(2)}) copy-start(bf16[2048,512]{1,0:T(8,128)(2,1)} %param.10) | copy-start | bytes 6291460
  4.7 9.3 %collective-permute-start = (bf16[192,128]{0,1:T(8,128)(2,1)S(1)}, bf16[192,128]{0,1:T(8,128)(2,1)S(1)}, u32[]{:S(2)}, u32[]{:S(2)}) collective-permute-start(bf16[192,128]{0,1:T(8,128)(2,1)S(1)} %pad_maximum_fusion), channel_id=1, source_target_pairs={{0,2},{2,4},{4,6},{6,8},{8,10},{10,12},{12,14},{14,0},{1,3},{3,5},... | collective-permute-start | bytes 147464 | tf_op jit(solution)/shard_map/ppermute | solution.py:65
  8.9 4.9 %copy-start.2 = (s32[1,6,32]{2,0,1:T(1,128)S(1)}, s32[1,6,32]{2,0,1:T(1,128)}, u32[]{:S(2)}) copy-start(s32[1,6,32]{2,0,1:T(1,128)} %param.9) | copy-start | bytes 2308
  9.0 4.9 %copy-start.3 = (s32[1,8]{1,0:T(1,128)S(1)}, s32[1,8]{1,0:T(1,128)}, u32[]{:S(2)}) copy-start(s32[1,8]{1,0:T(1,128)} %param.8) | copy-start | bytes 100
  14.1 7.0 %collective-permute-start.1 = (bf16[192,128]{0,1:T(8,128)(2,1)S(1)}, bf16[192,128]{0,1:T(8,128)(2,1)S(1)}, u32[]{:S(2)}, u32[]{:S(2)}) collective-permute-start(bf16[192,128]{0,1:T(8,128)(2,1)S(1)} %collective-permute-done), channel_id=1, source_target_pairs={{0,2},{2,4},{4,6},{6,8},{8,10},{10,12},{12,14},{14,0},{1,3},{3,5},... | collective-permute-start | bytes 147464 | tf_op jit(solution)/shard_map/ppermute | solution.py:65
  21.0 7.0 %collective-permute-start.2 = (bf16[192,128]{0,1:T(8,128)(2,1)S(1)}, bf16[192,128]{0,1:T(8,128)(2,1)S(1)}, u32[]{:S(2)}, u32[]{:S(2)}) collective-permute-start(bf16[192,128]{0,1:T(8,128)(2,1)S(1)} %collective-permute-done.1), channel_id=1, source_target_pairs={{0,2},{2,4},{4,6},{6,8},{8,10},{10,12},{12,14},{14,0},{1,3},{3,5},... | collective-permute-start | bytes 147464 | tf_op jit(solution)/shard_map/ppermute | solution.py:65
  28.0 7.0 %collective-permute-start.3 = (bf16[192,128]{0,1:T(8,128)(2,1)S(1)}, bf16[192,128]{0,1:T(8,128)(2,1)S(1)}, u32[]{:S(2)}, u32[]{:S(2)}) collective-permute-start(bf16[192,128]{0,1:T(8,128)(2,1)S(1)} %collective-permute-done.2), channel_id=1, source_target_pairs={{0,2},{2,4},{4,6},{6,8},{8,10},{10,12},{12,14},{14,0},{1,3},{3,5},... | collective-permute-start | bytes 147464 | tf_op jit(solution)/shard_map/ppermute | solution.py:65
  35.0 7.0 %collective-permute-start.4 = (bf16[192,128]{0,1:T(8,128)(2,1)S(1)}, bf16[192,128]{0,1:T(8,128)(2,1)S(1)}, u32[]{:S(2)}, u32[]{:S(2)}) collective-permute-start(bf16[192,128]{0,1:T(8,128)(2,1)S(1)} %collective-permute-done.3), channel_id=1, source_target_pairs={{0,2},{2,4},{4,6},{6,8},{8,10},{10,12},{12,14},{14,0},{1,3},{3,5},... | collective-permute-start | bytes 147464 | tf_op jit(solution)/shard_map/ppermute | solution.py:65
  41.9 7.5 %collective-permute-start.5 = (bf16[192,128]{0,1:T(8,128)(2,1)S(1)}, bf16[192,128]{0,1:T(8,128)(2,1)S(1)}, u32[]{:S(2)}, u32[]{:S(2)}) collective-permute-start(bf16[192,128]{0,1:T(8,128)(2,1)S(1)} %collective-permute-done.4), channel_id=1, source_target_pairs={{0,2},{2,4},{4,6},{6,8},{8,10},{10,12},{12,14},{14,0},{1,3},{3,5},... | collective-permute-start | bytes 147464 | tf_op jit(solution)/shard_map/ppermute | solution.py:65
  49.4 7.0 %collective-permute-start.6 = (bf16[192,128]{0,1:T(8,128)(2,1)S(1)}, bf16[192,128]{0,1:T(8,128)(2,1)S(1)}, u32[]{:S(2)}, u32[]{:S(2)}) collective-permute-start(bf16[192,128]{0,1:T(8,128)(2,1)S(1)} %collective-permute-done.5), channel_id=1, source_target_pairs={{0,2},{2,4},{4,6},{6,8},{8,10},{10,12},{12,14},{14,0},{1,3},{3,5},... | collective-permute-start | bytes 147464 | tf_op jit(solution)/shard_map/ppermute | solution.py:65
